TPU v7x, 256 devices: a whole 4x4x8 slice. The times are simulated.
256 devices in a mesh: ep: 16 (over y, x), tp: 16 (over z, core).
Axes of the slice: x: 4, y: 4, z: 8, core: 2. Of those that a mesh axis runs over, the one named last changes fastest.
Arguments:
- q_latent: bfloat16 [12288, 384], P(('ep', 'tp')), may hold values from -6 to 6
- kv_latent: bfloat16 [12288, 256], P(('ep', 'tp')), may hold values from -6 to 6
- rope_key: bfloat16 [12288, 64], P(('ep', 'tp')), may hold values from -6 to 6
- q_latent_gain: float32 [384], replicated, may hold values from 0.1 to 1.9
- kv_latent_gain: float32 [256], replicated, may hold values from 0.1 to 1.9
- w_query: bfloat16 [384, 3072], P(None, 'tp'), may hold values from -0.3125 to 0.3125
- w_key: bfloat16 [256, 2048], P(None, 'tp'), may hold values from -0.375 to 0.375
- w_value: bfloat16 [256, 2048], P(None, 'tp'), may hold values from -0.375 to 0.375
- query_gain: float32 [192], replicated, may hold values from 0.1 to 1.9
- key_gain: float32 [192], replicated, may hold values from 0.1 to 1.9
- w_mix: bfloat16 [2048, 2048], P('tp'), may hold values from -3 to 3
- tokens_b: bfloat16 [12288, 2048], P(('ep', 'tp')), may hold values from -6 to 6
- norm_gain: float32 [2048], replicated, may hold values from 0.1 to 1.9
- expert_ids: int32 [12288, 2], P(('ep', 'tp')), may hold values from 0 to 31, all different within a row; in each aligned block of 48 rows (0 to 47, 48 to 95, ...) at most 4 rows name the same one
- route_weights: float32 [12288, 2], P(('ep', 'tp')), may hold values from 0.05 to 1
- w_gate: bfloat16 [32, 2048, 4096], P('ep', None, 'tp'), may hold values from -0.125 to 0.125
- w_up: bfloat16 [32, 2048, 4096], P('ep', None, 'tp'), may hold values from -0.125 to 0.125
- w_down: bfloat16 [32, 4096, 2048], P('ep', 'tp'), may hold values from -0.09375 to 0.09375
Outputs:
- mix_out: bfloat16 [12288, 2048], P(('ep', 'tp'))
- expert_out: bfloat16 [12288, 2048], P(('ep', 'tp'))
Inputs may be any that keep to these rules, and one draw needn't show every extreme that they name: `expert_ids`: each row names 2 different experts. Within the rows of one device, no expert is named more than 4 times, a bound that some block reaches.
All inputs are finite; a program needn't handle non-finite values.
Results may differ from a plain program's by a relative error of at most 0.018.
Values may be sent and summed in bfloat16 or wider, within the bound.
A program may use at most 192 MiB of HBM per device.

v0:
```python
import jax
import jax.numpy as jnp
from jax import lax
from jax.sharding import PartitionSpec as P

NOPE_DIM = 128
ROPE_DIM = 64
VALUE_DIM = 128
EXPERTS = 32
TOP_K = 2


EPSILON = 1e-06
THETA = 10000.0


def sent_together(arrays, axis, dim, along):
    both = jnp.concatenate(arrays, axis=along)
    whole, at, outs = (lax.all_gather(both, axis, axis=dim, tiled=True), 0, [])
    for a in arrays:
        outs.append(lax.slice_in_dim(whole, at, at + a.shape[along], axis=along))
        at += a.shape[along]
    return tuple(outs)


def split_up(x, dim, peers):
    before, after = (x.shape[:dim], x.shape[dim + 1 :])
    return jnp.moveaxis(x.reshape(*before, peers, -1, *after), dim, 0)


def one_scatter(arrays, axis, dims):
    peers = lax.axis_size(axis)
    parts = [split_up(a, dim, peers) for a, dim in zip(arrays, dims)]
    lines = jnp.concatenate([b.reshape(peers, -1) for b in parts], axis=1)
    rows = max(16, -(-lines.shape[1] // 1024) * 8)
    lines = jnp.pad(lines, ((0, 0), (0, rows * 128 - lines.shape[1]))).reshape(-1, 128)
    ravelled, at, outs = (lax.psum_scatter(lines, axis, tiled=True).reshape(-1), 0, [])
    for b in parts:
        part = b[0]
        outs.append(ravelled[at : at + part.size].reshape(part.shape))
        at += part.size
    return tuple(outs)


def rms_scale(values, gains):
    return values * lax.rsqrt(jnp.mean(values * values, axis=-1, keepdims=True) + EPSILON) * gains


def rotate(values, positions):
    half_dim = values.shape[-1] // 2
    inverse = THETA ** (-jnp.arange(0, 2 * half_dim, 2, dtype=jnp.float32) / (2 * half_dim))
    angles = positions.astype(jnp.float32)[:, None] * inverse[None, :]
    view_shape = (positions.shape[0],) + (1,) * (values.ndim - 2) + (half_dim,)
    cosine = jnp.cos(angles).reshape(view_shape)
    sine_part = jnp.sin(angles).reshape(view_shape)
    first_half = values[..., :half_dim]
    second = values[..., half_dim:]
    return jnp.concatenate(
        [first_half * cosine - second * sine_part, second * cosine + first_half * sine_part],
        axis=-1,
    )


def attention(q_all, kv_all, rope_all, positions_q, w_query, w_key, w_value, query_gain, key_gain):
    rows_ep = q_all.shape[0]
    heads_dev = w_key.shape[1] // NOPE_DIM
    queries = jnp.dot(q_all, w_query, preferred_element_type=jnp.float32).reshape(
        rows_ep, heads_dev, NOPE_DIM + ROPE_DIM
    )
    queries = rms_scale(queries, query_gain)
    queries = jnp.concatenate(
        [queries[..., :NOPE_DIM], rotate(queries[..., NOPE_DIM:], positions_q)], axis=-1
    ).astype(jnp.bfloat16)
    score_scale = (NOPE_DIM + ROPE_DIM) ** (-0.5)
    latent, shared = sent_together((kv_all, rope_all), "ep", 0, 1)
    key_count = latent.shape[0]
    positions = jnp.arange(key_count, dtype=jnp.int32)
    keys = jnp.dot(latent, w_key, preferred_element_type=jnp.float32).reshape(
        key_count, heads_dev, NOPE_DIM
    )
    shared_rows = shared.astype(jnp.float32)[:, None, :]
    keys = rms_scale(jnp.concatenate([keys, shared_rows], axis=-1), key_gain)
    keys = jnp.concatenate(
        [keys[..., :NOPE_DIM], rotate(keys[..., NOPE_DIM:], positions)], axis=-1
    ).astype(jnp.bfloat16)
    values = jnp.dot(latent, w_value, preferred_element_type=jnp.float32).astype(jnp.bfloat16)
    values = values.reshape(key_count, heads_dev, VALUE_DIM)
    scores = (
        jnp.einsum("qhd,khd->hqk", queries, keys, preferred_element_type=jnp.float32) * score_scale
    )
    probs_f = jnp.exp(scores)
    totals = jnp.sum(probs_f, axis=-1)
    summed = jnp.einsum(
        "hqk,khv->hqv", probs_f.astype(jnp.bfloat16), values, preferred_element_type=jnp.float32
    )
    totals, summed = (totals, summed)
    return (summed / totals[..., None]).astype(jnp.bfloat16)


def expert_terms(pieces, w_gate, w_up, w_down):
    gate_pre = jnp.einsum("tsxcd,xdf->tsxcf", pieces, w_gate, preferred_element_type=jnp.float32)
    up_pre = jnp.einsum("tsxcd,xdf->tsxcf", pieces, w_up, preferred_element_type=jnp.float32)
    hidden = (jax.nn.silu(gate_pre) * up_pre).astype(jnp.bfloat16)
    return jnp.einsum("tsxcf,xfd->tsxcd", hidden, w_down, preferred_element_type=jnp.float32)


def on_device(
    q_latent,
    kv_latent,
    rope_key,
    q_latent_gain,
    kv_latent_gain,
    w_query,
    w_key,
    w_value,
    query_gain,
    key_gain,
    w_mix,
    tokens_b,
    norm_gain,
    expert_ids,
    route_weights,
    w_gate,
    w_up,
    w_down,
):
    tp_count = lax.axis_size("tp")
    ep_count = lax.axis_size("ep")
    local_rows = q_latent.shape[0]
    rows_ep = local_rows * tp_count
    width = tokens_b.shape[1]
    heads_dev = w_key.shape[1] // NOPE_DIM
    q_normed = rms_scale(q_latent.astype(jnp.float32), q_latent_gain).astype(jnp.bfloat16)
    kv_normed = rms_scale(kv_latent.astype(jnp.float32), kv_latent_gain).astype(jnp.bfloat16)
    positions_q = lax.axis_index("ep") * rows_ep + jnp.arange(rows_ep, dtype=jnp.int32)
    mix_weights = w_mix.reshape(heads_dev, VALUE_DIM, width)
    local_b = tokens_b.shape[0]
    capacity = max(2, local_b * TOP_K * 3 // (2 * EXPERTS))
    experts_dev = w_gate.shape[0]
    b_normed = rms_scale(tokens_b.astype(jnp.float32), norm_gain).astype(jnp.bfloat16)
    flat_ids = expert_ids.reshape(-1)
    expert_hot = (flat_ids[:, None] == jnp.arange(EXPERTS, dtype=jnp.int32)[None, :]).astype(
        jnp.int32
    )
    ranks = jnp.sum(expert_hot * (jnp.cumsum(expert_hot, axis=0) - 1), axis=1)
    slots = flat_ids * capacity + ranks
    slot_hot = (slots[:, None] == jnp.arange(EXPERTS * capacity, dtype=jnp.int32)[None, :]).astype(
        jnp.bfloat16
    )
    repeated = jnp.repeat(b_normed, TOP_K, axis=0)
    outgoing = jnp.einsum(
        "as,ad->sd", slot_hot, repeated, preferred_element_type=jnp.float32
    ).astype(jnp.bfloat16)
    outgoing = outgoing.reshape(ep_count, experts_dev * capacity, width)
    arrived = lax.all_to_all(outgoing, "ep", split_axis=0, concat_axis=0, tiled=True)
    arrived = arrived.reshape(1, ep_count, experts_dev, capacity, width)
    q_all, kv_all, rope_all, slots_all = (
        lax.all_gather(q_normed[None], "tp", axis=0, tiled=True),
        lax.all_gather(kv_normed[None], "tp", axis=0, tiled=True),
        lax.all_gather(rope_key[None], "tp", axis=0, tiled=True),
        lax.all_gather(arrived, "tp", axis=0, tiled=True),
    )
    head_out = attention(
        q_all.reshape(rows_ep, -1),
        kv_all.reshape(rows_ep, -1),
        rope_all.reshape(rows_ep, -1),
        positions_q,
        w_query,
        w_key,
        w_value,
        query_gain,
        key_gain,
    )
    mix_term = jnp.einsum("hqv,hvd->qd", head_out, mix_weights, preferred_element_type=jnp.float32)
    mix_term = mix_term.reshape(tp_count, local_rows, width)
    expert_term = expert_terms(slots_all, w_gate, w_up, w_down)
    mix_sum, expert_sum = tuple(
        (
            part.astype(jnp.float32)
            for part in one_scatter(
                (mix_term.astype(jnp.bfloat16), expert_term.astype(jnp.bfloat16)), "tp", (0, 0)
            )
        )
    )
    mix_out = mix_sum[0].astype(jnp.bfloat16)
    expert_done = expert_sum[0].astype(jnp.bfloat16)
    returning = expert_done.reshape(ep_count, experts_dev * capacity, width)
    returned = lax.all_to_all(returning, "ep", split_axis=0, concat_axis=0, tiled=True).reshape(
        EXPERTS * capacity, width
    )
    gathered_back = jnp.dot(slot_hot, returned, preferred_element_type=jnp.float32).reshape(
        local_b, TOP_K, width
    )
    expert_out = jnp.sum(gathered_back * route_weights[:, :, None], axis=1).astype(jnp.bfloat16)
    return (mix_out, expert_out)


def solution(mesh):
    in_specs = (
        P(("ep", "tp"), None),
        P(("ep", "tp"), None),
        P(("ep", "tp"), None),
        P(),
        P(),
        P(None, "tp"),
        P(None, "tp"),
        P(None, "tp"),
        P(),
        P(),
        P("tp", None),
        P(("ep", "tp"), None),
        P(),
        P(("ep", "tp"), None),
        P(("ep", "tp"), None),
        P("ep", None, "tp"),
        P("ep", None, "tp"),
        P("ep", "tp", None),
    )
    out_specs = (P(("ep", "tp"), None), P(("ep", "tp"), None))
    return jax.shard_map(
        on_device, mesh=mesh, in_specs=in_specs, out_specs=out_specs, check_vma=False
    )
```

profile of v0, /device:TPU:1, one launch (start us, length us, event | category | flops | bytes accessed | tf_op | source)
XLA Modules:
  0.0 367.1 jit_solution(14204939258254129752)
XLA Ops:
  7.3 1.0 fusion.69
  9.1 22.4 %all-gather.1 = bf16[768,256]{1,0:T(8,128)(2,1)S(1)} all-gather(bf16[48,256]{1,0:T(8,128)(2,1)S(1)} %fusion.71), channel_id=3, replica_groups=mesh['ep'=16,'tp'=16] {'tp'}, dimensions={0}, use_global_device_ids=true | all-gather | bytes 417792 | tf_op jit(solution)/shard_map/all_gather | solution.py:159
  31.6 15.2 %all-gather.2 = bf16[768,64]{1,0:T(8,128)(2,1)S(1)} all-gather(bf16[48,64]{1,0:T(8,128)(2,1)} %param.20), channel_id=4, replica_groups=mesh['ep'=16,'tp'=16] {'tp'}, dimensions={0}, use_global_device_ids=true | all-gather | bytes 104448 | tf_op jit(solution)/shard_map/all_gather | solution.py:160
  48.8 1.1 fusion.49
  49.8 1.1 fusion.51
  51.7 1.2 fusion.14
  53.0 6.8 %all-to-all-start = ((bf16[16,8,2048]{2,1,0:T(8,128)(2,1)}), bf16[16,8,2048]{2,1,0:T(8,128)(2,1)S(1)}, u32[]{:S(2)}, u32[]{:S(2)}) async-start(bf16[16,8,2048]{2,1,0:T(8,128)(2,1)} %fusion.14), calls=%async_computation | async-start | bytes 1048576 | tf_op jit(solution)/shard_map/all_to_all | solution.py:155
  60.0 17.7 %all-gather = bf16[768,384]{1,0:T(8,128)(2,1)S(1)} all-gather(bf16[48,384]{1,0:T(8,128)(2,1)S(1)} %fusion.68), channel_id=2, replica_groups=mesh['ep'=16,'tp'=16] {'tp'}, dimensions={0}, use_global_device_ids=true | all-gather | bytes 626688 | tf_op jit(solution)/shard_map/all_gather | solution.py:158
  78.7 1.1 copy.46
  79.9 42.8 %all-gather.6.cloned.1.call-done = bf16[12288,320]{0,1:T(8,128)(2,1)} async-done(((bf16[768,320]{0,1:T(8,128)(2,1)}), bf16[12288,320]{0,1:T(8,128)(2,1)}) %all-gather.6.cloned.1.call-update) | async-done | bytes 7864336 | tf_op jit(solution)/shard_map/all_gather | solution.py:19
  122.6 3.8 %convolution_bitcast_fusion = f32[12288,1,128]{0,2,1:T(8,128)S(1)} fusion(bf16[256,128]{1,0:T(8,128)(2,1)S(1)} %copy-done.6, bf16[12288,320]{0,1:T(8,128)(2,1)} %all-gather.6.cloned.1.call-done), kind=kOutput, calls=%fused_computation.5 | convolution fusion | flops 805306368 | bytes 12648448 | tf_op jit(solution)/shard_map/dot_general | solution.py:78
  126.5 2.9 fusion.36
  131.0 6.3 %convolution_convert_fusion = bf16[12288,128]{1,0:T(8,128)(2,1)} fusion(bf16[256,128]{1,0:T(8,128)(2,1)S(1)} %copy-done.12, bf16[12288,320]{0,1:T(8,128)(2,1)} %all-gather.6.cloned.1.call-done), kind=kOutput, calls=%fused_computation.6 | convolution fusion | flops 806879232 | bytes 9502720 | tf_op jit(solution)/shard_map/dot_general | solution.py:86
  137.3 8.7 %multiply_multiply_fusion = f32[12288,1,192]{0,2,1:T(8,128)} fusion(f32[12288,1,64]{0,2,1:T(8,128)} %copy-done.2, f32[12288,1,128]{0,2,1:T(8,128)} %copy-done.1, f32[192]{0:T(256)S(1)} %copy-done.9, f32[12288]{0:T(1024)S(1)} %add_rsqrt_fusion), kind=kLoop, calls=%fused_computation.9 | loop fusion | flops 7077888 | bytes 18924288 | tf_op jit(solution)/shard_map/mul | solution.py:46
  146.0 9.0 %fusion.46 = (bf16[12288,32]{0,1:T(8,128)(2,1)S(1)}, bf16[12288,32]{0,1:T(8,128)(2,1)}) fusion(f32[12288,1,192]{0,2,1:T(8,128)} %multiply_multiply_fusion, f32[32]{0:T(128)S(1)} %multiply_power_fusion, f32[12288]{0:T(1024)S(1)} %iota_convert_fusion), kind=kLoop, calls=%fused_computation.55 | loop fusion | flops 3538944 | bytes 4767872 | tf_op jit(solution)/shard_map/concatenate | solution.py:83
  155.1 4.9 %fusion.13 = bf16[12288,128]{0,1:T(8,128)(2,1)} fusion(f32[12288,1,192]{0,2,1:T(8,128)} %multiply_multiply_fusion), kind=kLoop, calls=%fused_computation.22 | loop fusion | bytes 6291456 | tf_op jit(solution)/shard_map/concatenate | solution.py:83
  160.0 17.3 %fusion = (f32[768]{0:T(1024)S(1)}, f32[768,12288]{1,0:T(8,128)}) fusion(bf16[12288,32]{0,1:T(8,128)(2,1)} %get-tuple-element.3, bf16[12288,32]{0,1:T(8,128)(2,1)S(1)} %get-tuple-element.2, bf16[12288,128]{0,1:T(8,128)(2,1)} %fusion.13, bf16[768,32]{0,1:T(8,128)(2,1)S(1)} %get-tuple-element.5, bf16[768,32]{0,1:T(8,128)(2,1)S(1)} %get-tuple-element.4, ...), kind=kOutput, calls=%fused_computation.1 | convolution fusion | flops 3657792768 | bytes 42765312 | tf_op jit(solution)/shard_map/qhd,khd->hqk/dot_general | solution.py:89
  177.3 15.4 %fusion.41 = bf16[768,128]{1,0:T(8,128)(2,1)S(1)} fusion(bf16[12288,128]{1,0:T(8,128)(2,1)} %convolution_convert_fusion, f32[768,12288]{1,0:T(8,128)} %get-tuple-element.9, f32[768]{0:T(1024)S(1)} %get-tuple-element.8), kind=kOutput, calls=%fused_computation.52 | convolution fusion | flops 2434990080 | bytes 41094144 | tf_op jit(solution)/shard_map/hqk,khv->hqv/dot_general | solution.py:93
  192.8 1.0 convolution_convert_fusion.1
  193.7 3.5 copy.52
  197.2 7.6 %fusion.20 = f32[2,16,16,4,256]{4,2,3,1,0:T(8,128)} fusion(bf16[16,16,2,4,2048]{4,1,3,0,2:T(8,128)(2,1)} %all-gather.8.cloned.1.call-done, bf16[2,2048,256]{2,1,0:T(8,128)(2,1)} %param.34), kind=kOutput, calls=%fused_computation.33 | convolution fusion | flops 2147483648 | bytes 12582912 | tf_op jit(solution)/shard_map/tsxcd,xdf->tsxcf/dot_general | solution.py:102
  204.8 13.5 %convert_bitcast_fusion = bf16[16,16,2,4,2048]{4,1,3,0,2:T(8,128)(2,1)} fusion(bf16[2,256,2048]{2,1,0:T(8,128)(2,1)S(1)} %copy-done, f32[2,16,16,4,256]{4,2,3,1,0:T(8,128)} %fusion.20, bf16[16,16,2,4,2048]{4,1,3,0,2:T(8,128)(2,1)} %all-gather.8.cloned.1.call-done, bf16[2,2048,256]{2,1,0:T(8,128)(2,1)} %param.33), kind=kOutput, calls=%fused_computation.11 | convolution fusion | flops 4302307328 | bytes 23068672 | tf_op jit(solution)/shard_map/tsxcf,xfd->tsxcd/dot_general | solution.py:104
  218.3 11.1 %copy.47 = bf16[16,16,2,4,2048]{4,3,2,1,0:T(4,128)(2,1)} copy(bf16[16,16,2,4,2048]{4,1,3,0,2:T(8,128)(2,1)} %convert_bitcast_fusion) | data formatting | bytes 16777216 | tf_op jit(solution)/shard_map/convert_element_type | solution.py:181
  229.4 10.3 %reshape_reshape.7 = bf16[16,262144]{1,0:T(8,128)(2,1)} reshape(bf16[16,16,2,4,2048]{4,3,2,1,0:T(4,128)(2,1)} %copy.47) | data formatting | bytes 16777216 | tf_op jit(solution)/shard_map/reshape;reshape | solution.py:34
  239.7 12.5 %pad_maximum_fusion = bf16[16,360448]{1,0:T(8,128)(2,1)} fusion(bf16[16,262144]{1,0:T(8,128)(2,1)} %reshape_reshape.7, bf16[16,98304]{1,0:T(8,128)(2,1)} %bitcast.90), kind=kLoop, calls=%fused_computation.7 | loop fusion | flops 23068672 | bytes 23068672 | tf_op jit(solution)/shard_map/concatenate | solution.py:34
  252.1 15.4 %reshape.518 = bf16[45056,128]{1,0:T(8,128)(2,1)} reshape(bf16[16,360448]{1,0:T(8,128)(2,1)} %pad_maximum_fusion) | data formatting | bytes 23068672 | tf_op jit(solution)/shard_map/reshape | solution.py:36
  267.6 74.4 %reduce-scatter.2.cloned.1.call-done = bf16[2816,128]{1,0:T(8,128)(2,1)} async-done(((bf16[45056,128]{1,0:T(8,128)(2,1)}), bf16[2816,128]{1,0:T(8,128)(2,1)}) %reduce-scatter.2.cloned.1.call-update) | async-done | bytes 720912 | tf_op jit(solution)/shard_map/reduce_scatter | solution.py:37
  342.0 1.1 slice.59
  343.1 1.0 reshape.520
  344.1 6.5 %all-to-all-start.1 = ((bf16[16,8,2048]{2,1,0:T(8,128)(2,1)}), bf16[16,8,2048]{2,1,0:T(8,128)(2,1)S(1)}, u32[]{:S(2)}, u32[]{:S(2)}) async-start(bf16[16,8,2048]{2,1,0:T(8,128)(2,1)} %reshape.520), calls=%async_computation.2 | async-start | bytes 1048576 | tf_op jit(solution)/shard_map/all_to_all | solution.py:188
  352.5 7.1 %all-to-all-done.1 = bf16[16,8,2048]{2,1,0:T(8,128)(2,1)S(1)} async-done(((bf16[16,8,2048]{2,1,0:T(8,128)(2,1)}), bf16[16,8,2048]{2,1,0:T(8,128)(2,1)S(1)}, u32[]{:S(2)}, u32[]{:S(2)}) %all-to-all-start.1) | async-done | bytes 524320 | tf_op jit(solution)/shard_map/all_to_all | solution.py:188
  359.6 1.0 fusion.37
  (66 shorter events, 8.6 us)
Async XLA Ops:
  7.2 197.7 %copy-start = (bf16[2,256,2048]{2,1,0:T(8,128)(2,1)S(1)}, bf16[2,256,2048]{2,1,0:T(8,128)(2,1)}, u32[]{:S(2)}) copy-start(bf16[2,256,2048]{2,1,0:T(8,128)(2,1)} %param.35) | copy-start | bytes 6291460
  7.2 52.6 %copy-start.4 = (bf16[48,384]{1,0:T(8,128)(2,1)S(1)}, bf16[48,384]{1,0:T(8,128)(2,1)}, u32[]{:S(2)}) copy-start(bf16[48,384]{1,0:T(8,128)(2,1)} %param.18) | copy-start | bytes 110596
  7.2 52.7 %copy-start.8 = (f32[384]{0:T(512)S(1)}, f32[384]{0:T(512)}, u32[]{:S(2)}) copy-start(f32[384]{0:T(512)} %param.21) | copy-start | bytes 4612
  7.2 70.5 %copy-start.5 = (bf16[384,192]{0,1:T(8,128)(2,1)S(1)}, bf16[384,192]{0,1:T(8,128)(2,1)}, u32[]{:S(2)}) copy-start(bf16[384,192]{0,1:T(8,128)(2,1)} %param.23) | copy-start | bytes 442372
  7.2 70.9 %copy-start.11 = (f32[192]{0:T(256)S(1)}, f32[192]{0:T(256)}, u32[]{:S(2)}) copy-start(f32[192]{0:T(256)} %param.26) | copy-start | bytes 2308
  7.2 115.4 %all-gather.6.cloned.1.call-start = ((), (), s32[]{:S(2)}) async-start(), calls=%async_computation.3 | async-start | bytes 8355840 | tf_op jit(solution)/shard_map/all_gather | solution.py:19
  31.5 91.2 %copy-start.6 = (bf16[256,128]{1,0:T(8,128)(2,1)S(1)}, bf16[256,128]{1,0:T(8,128)(2,1)}, u32[]{:S(2)}) copy-start(bf16[256,128]{1,0:T(8,128)(2,1)} %param.24) | copy-start | bytes 196612
  53.0 25.7 %all-to-all-start = ((bf16[16,8,2048]{2,1,0:T(8,128)(2,1)}), bf16[16,8,2048]{2,1,0:T(8,128)(2,1)S(1)}, u32[]{:S(2)}, u32[]{:S(2)}) async-start(bf16[16,8,2048]{2,1,0:T(8,128)(2,1)} %fusion.14), calls=%async_computation | async-start | bytes 1048576 | tf_op jit(solution)/shard_map/all_to_all | solution.py:155
  59.7 137.5 %all-gather.8.cloned.1.call-start = ((), (), s32[]{:S(2)}) async-start(), calls=%async_computation.4 | async-start | bytes 8912896 | tf_op jit(solution)/shard_map/all_gather | solution.py:161
  79.8 262.2 %reduce-scatter.2.cloned.1.call-start = ((), (), s32[]{:S(2)}) async-start(), calls=%async_computation.5 | async-start | bytes 12255232 | tf_op jit(solution)/shard_map/reduce_scatter | solution.py:37
  126.5 3.7 %copy-start.1 = (f32[12288,1,128]{0,2,1:T(8,128)}, f32[12288,1,128]{0,2,1:T(8,128)S(1)}, u32[]{:S(2)}) copy-start(f32[12288,1,128]{0,2,1:T(8,128)S(1)} %convolution_bitcast_fusion) | copy-start | bytes 18874372
  126.5 4.5 %copy-start.12 = (bf16[256,128]{1,0:T(8,128)(2,1)S(1)}, bf16[256,128]{1,0:T(8,128)(2,1)}, u32[]{:S(2)}) copy-start(bf16[256,128]{1,0:T(8,128)(2,1)} %param.25) | copy-start | bytes 196612
  129.4 1.7 copy-start.2
  131.0 6.3 %copy-start.9 = (f32[192]{0:T(256)S(1)}, f32[192]{0:T(256)}, u32[]{:S(2)}) copy-start(f32[192]{0:T(256)} %param.27) | copy-start | bytes 2308
  177.3 15.4 %copy-start.3 = (bf16[128,2048]{1,0:T(8,128)(2,1)S(1)}, bf16[128,2048]{1,0:T(8,128)(2,1)}, u32[]{:S(2)}) copy-start(bf16[128,2048]{1,0:T(8,128)(2,1)} %param.28) | copy-start | bytes 1572868
  267.5 83.3 %copy-start.7 = (s32[48,2]{0,1:T(2,128)S(1)}, s32[48,2]{0,1:T(2,128)}, u32[]{:S(2)}) copy-start(s32[48,2]{0,1:T(2,128)} %param.31) | copy-start | bytes 1156
  267.5 92.1 %copy-start.10 = (f32[48,2]{0,1:T(2,128)S(1)}, f32[48,2]{0,1:T(2,128)}, u32[]{:S(2)}) copy-start(f32[48,2]{0,1:T(2,128)} %param.32) | copy-start | bytes 1156
  344.1 15.5 %all-to-all-start.1 = ((bf16[16,8,2048]{2,1,0:T(8,128)(2,1)}), bf16[16,8,2048]{2,1,0:T(8,128)(2,1)S(1)}, u32[]{:S(2)}, u32[]{:S(2)}) async-start(bf16[16,8,2048]{2,1,0:T(8,128)(2,1)} %reshape.520), calls=%async_computation.2 | async-start | bytes 1048576 | tf_op jit(solution)/shard_map/all_to_all | solution.py:188
Sparse Core Ops, SparseCore 0:
  48.0 74.6 all-gather.5
  124.5 56.1 all-gather.7
  267.7 74.2 reduce-scatter.1
where the time goes:
time: 370 us; the launch traced here: 367 us
  waiting for transfers between devices  124 us (34%)
  matrix products  67.5 us (18%)
  blocking collectives  55.3 us (15%)
  local copies, waits for them, and re-layouts  52.7 us (14%)
  other arithmetic  39.8 us (11%)
  between operations  14.1 us (4%)
  starting transfers between devices  13.4 us (4%)
    reduce_scatter x1, waiting for transfers between devices, one_scatter(): lax.psum_scatter(lines, axis, tiled=True).reshape(-1)  74.4 us
    all_gather x1, waiting for transfers between devices, sent_together(): whole, at, outs = (lax.all_gather(both, axis, axis=dim, tiled=True), 0, [])  42.8 us
    all_gather x1, blocking collectives, on_device(): lax.all_gather(kv_normed[None], 'tp', axis=0, tiled=True)  22.4 us
    all_gather x1, blocking collectives, on_device(): lax.all_gather(q_normed[None], 'tp', axis=0, tiled=True)  17.7 us
    dot_general x1, matrix products, attention(): jnp.einsum('qhd,khd->hqk', queries, keys, preferred_element_type=jnp.floa...  17.3 us
    dot_general x1, matrix products, attention(): jnp.einsum('hqk,khv->hqv', probs_f.astype(jnp.bfloat16), values, preferre...  15.4 us
    reshape x1, local copies, waits for them, and re-layouts, one_scatter(): jnp.pad(lines, ((0, 0), (0, rows * 128 - lines.shape[1]))).reshape(-1, 128)  15.4 us
    all_gather x1, blocking collectives, on_device(): lax.all_gather(rope_key[None], 'tp', axis=0, tiled=True)  15.2 us
  transfers between devices with their start and end apart: 5, of which 3 were waited for; matrix products, arithmetic and copies ran while one was open for 23% of the time, Pallas kernels for 0%

commit v1 on v0

v1 whole, which is shorter than its diff:
```python
import jax
import jax.numpy as jnp
import numpy as np
from jax import lax
from jax.experimental import pallas as pl
from jax.experimental.pallas import tpu as pltpu
from jax.sharding import PartitionSpec as P

F32, BF16 = jnp.float32, jnp.bfloat16
MESH = pl.DeviceIdType.MESH
EPSILON = 1e-06
THETA = 10000.0
LOG2E = 1.4426950408889634
SCORE = 192 ** (-0.5)
NT = (((1,), (1,)), ((), ()))
TN = (((0,), (0,)), ((), ()))
HALF = 64


def rope_tables():
    inverse = THETA ** (-np.arange(0, 64, 2, dtype=np.float64) / 64)
    rows = np.arange(768).reshape(8, 2, 48).transpose(1, 0, 2).reshape(768)
    angle = np.tile(rows[:, None] * inverse[None, :], (1, 2))
    base = np.concatenate([np.cos(angle), np.sin(angle)], axis=1).astype(np.float32)
    offset = np.tile((np.arange(16) * 768)[:, None] * inverse[None, :], (1, 4))
    shift = np.stack([np.cos(offset), np.sin(offset)], axis=1).astype(np.float32)
    return base.reshape(16, 48, 128), shift.reshape(16, 2, 128)


def send(src, dst, send_sem, recv_sem, device):
    pltpu.make_async_remote_copy(
        src_ref=src, dst_ref=dst, send_sem=send_sem, recv_sem=recv_sem, device_id=device, device_id_type=MESH
    ).start()


def await_bytes(ref, sem):
    pltpu.make_async_copy(ref, ref, sem).wait()


def normed(x, gain):
    return x * lax.rsqrt(jnp.mean(x * x, axis=-1, keepdims=True) + EPSILON) * gain


def layer(
    ql_ref, kvl_ref, rope_ref, vec_ref, wq_ref, wkv_ref, tokens_ref, ids_ref, route_ref, base_ref, shift_ref,
    wmix_hbm, wg_hbm, wu_hbm, wd_hbm,
    mix_ref, expert_ref,
    wmix, wg, wu, wd, qg, queries, acc, lg, st, outgoing, arrived, returned, xg, pg, sg, rr, rl, mp, msg, mr, ml,
    w_sem, z_sem, q_sib, la, lb, ls, a2a, ret, xr, xl, xs_own, xs_r, xs_l, sgs, rrs, rls, ms, mrs, mls, out_sem,
):
    e, t = lax.axis_index("ep"), lax.axis_index("tp")
    z, c = t // 2, t % 2
    other = 1 - c
    sib = (e, z * 2 + other)

    def zpeer(d):
        return (e, ((z + d) % 8) * 2 + c)

    right, left = zpeer(1), zpeer(7)
    ey, ex = e // 4, e % 4
    pa = other * ex + c * ey
    pb = other * ey + c * ex

    def origin(da, db):
        a, b = (pa + da + 4) % 4, (pb + db + 4) % 4
        return other * (b * 4 + a) + c * (a * 4 + b)

    barrier = pltpu.get_barrier_semaphore()
    for d in range(1, 8):
        pl.semaphore_signal(barrier, inc=1, device_id=zpeer(d), device_id_type=MESH)
    for d in range(1, 16):
        pl.semaphore_signal(barrier, inc=1, device_id=((e + d) % 16, t), device_id_type=MESH)
    pl.semaphore_signal(barrier, inc=1, device_id=sib, device_id_type=MESH)

    loads = [
        pltpu.make_async_copy(src, dst, w_sem.at[n])
        for n, (src, dst) in enumerate([(wg_hbm, wg), (wu_hbm, wu), (wd_hbm, wd), (wmix_hbm, wmix)])
    ]
    for load in loads:
        load.start()

    ids = ids_ref[...]
    experts = lax.broadcasted_iota(jnp.int32, (48, 32), 1)
    hot = [(ids[:, k : k + 1] == experts).astype(F32) for k in range(2)]
    lower = (
        lax.broadcasted_iota(jnp.int32, (48, 48), 0) > lax.broadcasted_iota(jnp.int32, (48, 48), 1)
    ).astype(BF16)
    before = [jnp.dot(lower, h.astype(BF16), preferred_element_type=F32) for h in hot]
    before[1] = before[1] + jnp.sum(hot[0], axis=0, keepdims=True)
    places = lax.broadcasted_iota(jnp.int32, (48, 128), 1).astype(F32)
    for k in range(2):
        rank = jnp.sum(hot[k] * before[k], axis=1, keepdims=True)
        slot = ids[:, k : k + 1].astype(F32) * 4.0 + rank
        st[k] = (slot == places).astype(BF16)
    b_normed = normed(tokens_ref[...].astype(F32), vec_ref[:, 1152:3200]).astype(BF16)
    slots = lax.dot_general(st[0] + st[1], b_normed, TN, preferred_element_type=F32)
    slots = slots.reshape(16, 8, 2048)
    outgoing[...] = jnp.concatenate([slots[:, :, :1024], slots[:, :, 1024:]], axis=1).astype(BF16)

    trig_q = shift_ref[pl.ds(e, 1), 0], shift_ref[pl.ds(e, 1), 1]
    lane = lax.broadcasted_iota(jnp.int32, (1, 128), 1)
    flip = jnp.where(lane < 64, -1.0, 1.0)

    def turning(u, gains):
        return (trig_q[0] * u + trig_q[1] * (pltpu.roll(u, 64, axis=1) * flip)) * gains

    def turned(v):
        return v + pltpu.roll(v, 64, axis=1)

    qg[c, z] = normed(ql_ref[...].astype(F32), vec_ref[:, 0:384]).astype(BF16)
    mine = lg.at[e * 2 + c, z]
    mine[:, 0:256] = normed(kvl_ref[...].astype(F32), vec_ref[:, 384:640]).astype(BF16)
    rope = rope_ref[...].astype(F32)
    rope_rot = turned(rope * turning(base_ref[c * 8 + z], vec_ref[:, 1024:1152]))
    squares = jnp.sum(jnp.where(lane < 64, rope * rope, 0.0), axis=1, keepdims=True)
    high = squares.astype(BF16).astype(F32)
    mine[:, 256:384] = jnp.where(
        lane < 64, rope_rot, jnp.where(lane == 64, high, jnp.where(lane == 65, squares - high, 0.0))
    ).astype(BF16)

    pl.semaphore_wait(barrier, 23)
    for d in range(1, 16):
        peer = (e + d) % 16
        send(outgoing.at[peer], arrived.at[e], out_sem.at[0], a2a, (peer, t))
    for d in range(1, 8):
        send(mine, mine, out_sem.at[1], z_sem.at[0], zpeer(d))
    for d in range(1, 8):
        send(qg.at[c, z], qg.at[c, z], out_sem.at[2], z_sem.at[1], zpeer(d))
    arrived[pl.ds(e, 1)] = outgoing[pl.ds(e, 1)]

    a_up, a_down = (origin(1, 0), t), (origin(-1, 0), t)
    b_up, b_down = (origin(0, 1), t), (origin(0, -1), t)

    def block(da, db):
        return lg.at[origin(da, db) * 2 + c]

    def part(da, db, n):
        return lg.at[origin(da, db) * 2 + c, pl.ds(4 * n, 4)]

    def full(ref, sem, device):
        send(ref, ref, out_sem.at[3], sem, device)

    def along_b(n, da):
        full(block(da, 0), lb.at[n, 0], b_up)
        full(block(da, 0), lb.at[n, 1], b_down)
        full(block(da, 0), ls, sib)

    def start_latents():
        await_bytes(lg.at[0, pl.ds(0, 7)], z_sem.at[0])
        full(block(0, 0), la.at[0], a_up)
        full(block(0, 0), la.at[1], a_down)
        along_b(0, 0)

    def relay_a():
        await_bytes(block(-1, 0), la.at[0])
        full(part(-1, 0, 0), la.at[2], a_up)
        along_b(1, -1)
        await_bytes(block(1, 0), la.at[1])
        full(part(1, 0, 1), la.at[3], a_down)
        along_b(2, 1)

    def relay_a_far():
        await_bytes(part(2, 0, 0), la.at[2])
        await_bytes(part(2, 0, 1), la.at[3])
        along_b(3, 2)

    def relay_b(n):
        da = (0, -1, 1, 2)[n]
        await_bytes(block(da, -1), lb.at[n, 0])
        full(part(da, -1, 0), lb.at[n, 2], b_up)
        full(block(da, -1), ls, sib)
        await_bytes(block(da, 1), lb.at[n, 1])
        full(part(da, 1, 1), lb.at[n, 3], b_down)
        full(block(da, 1), ls, sib)

    def relay_b_far(n):
        da = (0, -1, 1, 2)[n]
        await_bytes(part(da, 2, 0), lb.at[n, 2])
        await_bytes(part(da, 2, 1), lb.at[n, 3])
        full(block(da, 2), ls, sib)

    def start_queries():
        await_bytes(qg.at[0, pl.ds(0, 7)], z_sem.at[1])
        send(qg.at[c], qg.at[c], out_sem.at[4], q_sib, sib)

    def make_queries():
        await_bytes(qg.at[0], q_sib)

        def rows(n, carry):
            x = qg[n // 2, pl.ds((n % 2) * 4, 4)].reshape(192, 384)
            p = jnp.dot(x, wq_ref[...], preferred_element_type=F32)
            nope, rot = p[:, :128], p[:, 128:]
            total = jnp.sum(nope * nope + jnp.where(lane < 64, rot * rot, 0.0), axis=1, keepdims=True)
            scale = lax.rsqrt(total * (1.0 / 192.0) + EPSILON) * (SCORE * LOG2E)
            angles = turning(base_ref[pl.ds(n * 4, 4)].reshape(192, 128), vec_ref[:, 768:896])
            rot = jnp.where(lane < 64, turned(rot * angles), 0.0) * scale
            at = pl.ds(pl.multiple_of(n * 192, 192), 192)
            queries[at, 0:128] = (nope * vec_ref[:, 640:768] * scale).astype(BF16)
            queries[at, 128:256] = rot.astype(BF16)
            acc[at] = jnp.zeros((192, 256), F32)
            return carry

        lax.fori_loop(0, 4, rows, 0)

    def attend(first, last):
        def keys_of(n, carry):
            rows = lg[n].reshape(384, 384)
            kv = jnp.dot(rows[:, :256], wkv_ref[...], preferred_element_type=F32)
            tail = rows[:, 256:].astype(F32)
            nope = kv[:, :128]
            total = jnp.sum(nope * nope + jnp.where(lane < 64, 0.0, tail), axis=1, keepdims=True)
            scale = lax.rsqrt(total * (1.0 / 192.0) + EPSILON)
            keys = jnp.concatenate(
                [nope * (vec_ref[:, 896:1024] * scale), jnp.where(lane < 64, tail, 0.0) * scale], axis=1
            ).astype(BF16)
            values = jnp.concatenate([kv[:, 128:].astype(BF16), jnp.ones((384, 128), BF16)], axis=1)
            for m in range(3):
                at = pl.ds(m * 256, 256)
                scores = lax.dot_general(queries[at], keys, NT, preferred_element_type=F32)
                acc[at] += jnp.dot(jnp.exp2(scores).astype(BF16), values, preferred_element_type=F32)
            return carry

        lax.fori_loop(first, last, keys_of, 0)

    def xblock(zo, h, core):
        return xg.at[(zo * 2 + h) * 2 + core]

    def xsend(ref, sem, device):
        send(ref, ref, out_sem.at[5], sem, device)

    def settle():
        await_bytes(outgoing.at[pl.ds(0, 15)], a2a)
        row = lax.broadcasted_iota(jnp.int32, (128, 128), 0)
        col = lax.broadcasted_iota(jnp.int32, (128, 128), 1)
        moved = (row == (col % 8 // 4) * 64 + col // 8 * 4 + col % 4).astype(BF16)
        came = arrived[...].astype(F32)
        for n in range(2):
            piece = came[:, n * 8 : n * 8 + 8].reshape(128, 1024).astype(BF16)
            piece = jnp.dot(moved, piece, preferred_element_type=F32).astype(BF16)
            for h in range(2):
                xg[(z * 2 + h) * 2 + c, :, n * 1024 : n * 1024 + 1024] = piece[h * HALF : h * HALF + HALF]
        for h in range(2):
            xsend(xblock(z, h, c), xr.at[h], right)
            xsend(xblock(z, h, c), xl.at[h], left)
            xsend(xblock(z, h, c), xs_own.at[h], sib)

    def relay_rows(j):
        k, hr = j // 2 + 1, j % 2
        hl = hr + j // 6
        from_left, from_right = xblock((z - k + 8) % 8, hr, c), xblock((z + k) % 8, hl, c)
        await_bytes(from_left, xr.at[j])

        @pl.when(j <= 4)
        def _():
            xsend(from_left, xr.at[j + 2], right)

        xsend(from_left, xs_r.at[j], sib)
        await_bytes(from_right, xl.at[j])

        @pl.when(j <= 3)
        def _():
            xsend(from_right, xl.at[j + 2], left)

        @pl.when(j == 5)
        def _():
            xsend(from_right, xl.at[6], left)

        xsend(from_right, xs_l.at[j], sib)

    def expert(zo, h, sem):
        x = xg[pl.ds((zo * 2 + h) * 2, 2)].reshape(128, 2048)
        gate = jnp.dot(x, wg[h], preferred_element_type=F32)
        up = jnp.dot(x, wu[h], preferred_element_type=F32)
        hidden = (gate / (1.0 + jnp.exp(-gate)) * up).astype(BF16)
        for n in range(4):
            cols = pl.ds(n * 512, 512)
            y = jnp.dot(hidden, wd[h, :, cols], preferred_element_type=F32).astype(BF16)
            pg[zo * 2 + h, :, cols] = y[:HALF]
            pg[16 + zo * 2 + h, :, cols] = y[HALF:]
        send(pg.at[other * 16 + zo * 2 + h], sg.at[zo * 2 + h], out_sem.at[6], sem, sib)

    def expert_pair(i):
        j = i - 1
        k = (j + 2) // 2
        h0 = (1 - (i + 7) // 8) * 0 + ((i + 7) // 8) * (j + 2) % 2
        started = (i + 7) // 8

        @pl.when(i == 0)
        def _():
            await_bytes(xblock(z, 0, other), xs_own.at[0])
            await_bytes(xblock(z, 1, other), xs_own.at[1])

        @pl.when(i > 0)
        def _():
            await_bytes(xblock((z - k + 8) % 8, 0, other), xs_r.at[j])
            await_bytes(xblock((z + k) % 8, 0, other), xs_l.at[j])

        def one(s, carry):
            zo = (z + started * (s * k + (1 - s) * (8 - k))) % 8
            hs = (1 - started) * s + started * (h0 + s * (i // 7))
            expert(zo, hs, sgs.at[i * 2 + s])
            return carry

        lax.fori_loop(0, 2, one, 0)

    def add_rows(out, terms, rows):
        def tile(n, carry):
            at = pl.ds(pl.multiple_of(n * 16, 16), 16)
            total = terms[0][at].astype(F32)
            for term in terms[1:]:
                total += term[at].astype(F32)
            out[at] = total.astype(BF16)
            return carry

        lax.fori_loop(0, rows // 16, tile, 0)

    def sums_event(m):
        k = 4 - (m + 1) // 2
        for side in range(2):
            h = m % 2 if side == 0 else 1 - m % 2
            zo = (z + k) % 8 if side == 0 else (z + 8 - k) % 8
            step = 2 * (k - 1) + h + 1 if k < 4 else 7
            which = (1 - side) if k < 4 else side
            await_bytes(sg.at[zo * 2 + h], sgs.at[step * 2 + which])
            mine_, recv, sems, device = (pg.at[c * 16 + zo * 2 + h], (rr, rl)[side], (rrs, rls)[side], (right, left)[side])
            terms = [mine_, sg.at[zo * 2 + h]]
            if m >= 2:
                await_bytes(recv.at[m - 2], sems.at[m - 2])
                terms.append(recv.at[m - 2])
            add_rows(mine_, terms, HALF)
            send(mine_, recv.at[m], out_sem.at[7], sems.at[m], device)

    def sums_final():
        for h in range(2):
            await_bytes(sg.at[z * 2 + h], sgs.at[h])
            await_bytes(rr.at[6 - h], rrs.at[6 - h])
            await_bytes(rl.at[5 + h], rls.at[5 + h])
            own = pg.at[c * 16 + z * 2 + h]
            add_rows(own, [own, sg.at[z * 2 + h], rr.at[6 - h], rl.at[5 + h]], HALF)
        row = lax.broadcasted_iota(jnp.int32, (128, 128), 0)
        col = lax.broadcasted_iota(jnp.int32, (128, 128), 1)
        back = (col == (row % 8 // 4) * 64 + row // 8 * 4 + row % 4).astype(BF16)
        done = pg[pl.ds(c * 16 + z * 2, 2)].reshape(128, 2048)
        rows = jnp.dot(back, done, preferred_element_type=F32).reshape(16, 8, 2048)
        arrived[...] = jnp.concatenate([rows[:, :, :1024], rows[:, :, 1024:]], axis=1).astype(BF16)
        for d in range(1, 16):
            peer = (e + d) % 16
            send(arrived.at[peer], returned.at[e], out_sem.at[8], ret, (peer, t))
        returned[pl.ds(e, 1)] = arrived[pl.ds(e, 1)]

    def project():
        def piece(n, carry):
            core, quarter = n // 4, n % 4
            at = pl.ds(pl.multiple_of(core * 384, 384), 384)
            block_ = acc[at]
            heads = (block_[:, :128] / block_[:, 128:]).astype(BF16)
            y = jnp.dot(
                heads, wmix[:, pl.ds(pl.multiple_of(quarter * 512, 512), 512)], preferred_element_type=F32
            ).astype(BF16)
            for zo in range(8):
                mp[core * 16 + zo * 2 + quarter // 2, :, pl.ds(pl.multiple_of(quarter % 2 * 512, 512), 512)] = y[
                    zo * 48 : zo * 48 + 48
                ]
            return carry

        lax.fori_loop(0, 8, piece, 0)
        send(mp.at[pl.ds(other * 16, 16)], msg, out_sem.at[9], ms, sib)

    def mix_event(m):
        k = 4 - (m + 1) // 2
        if m == 0:
            await_bytes(msg, ms)
        for side in range(2):
            h = m % 2 if side == 0 else 1 - m % 2
            zo = (z + k) % 8 if side == 0 else (z + 8 - k) % 8
            mine_, recv, sems, device = (mp.at[c * 16 + zo * 2 + h], (mr, ml)[side], (mrs, mls)[side], (right, left)[side])
            terms = [mine_, msg.at[zo * 2 + h]]
            if m >= 2:
                await_bytes(recv.at[m - 2], sems.at[m - 2])
                terms.append(recv.at[m - 2])
            add_rows(mine_, terms, 48)
            send(mine_, recv.at[m], out_sem.at[10], sems.at[m], device)

    def mix_final():
        for h in range(2):
            await_bytes(mr.at[6 - h], mrs.at[6 - h])
            await_bytes(ml.at[5 + h], mls.at[5 + h])
            add_rows(
                mix_ref.at[:, pl.ds(h * 1024, 1024)],
                [mp.at[c * 16 + z * 2 + h], msg.at[z * 2 + h], mr.at[6 - h], ml.at[5 + h]],
                48,
            )

    def combine():
        await_bytes(outgoing.at[pl.ds(0, 15)], ret)
        came = returned[...].astype(F32)
        for n in range(2):
            piece = came[:, n * 8 : n * 8 + 8].reshape(128, 1024).astype(BF16)
            total = jnp.zeros((48, 1024), F32)
            for k in range(2):
                total += jnp.dot(st[k], piece, preferred_element_type=F32) * route_ref[:, k : k + 1]
            expert_ref[:, n * 1024 : n * 1024 + 1024] = total.astype(BF16)

    start_latents()
    start_queries()
    settle()
    for load in loads:
        load.wait()

    def step(i, carry):
        @pl.when(i == 0)
        def _():
            relay_a()
            make_queries()

        @pl.when(i > 0)
        def _():
            relay_rows(i - 1)

        @pl.when(i == 1)
        def _():
            relay_a_far()
            relay_b(0)

        @pl.when(i == 2)
        def _():
            relay_b_far(0)
            relay_b(1)

        @pl.when(i == 3)
        def _():
            relay_b_far(1)
            relay_b(2)

        @pl.when(i == 4)
        def _():
            relay_b_far(2)
            relay_b(3)

        @pl.when(i == 5)
        def _():
            relay_b_far(3)
            await_bytes(lg.at[pl.ds(0, 16)], ls)

        @pl.when(i > 0)
        def _():
            expert_pair(i - 1)

        @pl.when(i >= 6)
        def _():
            attend((i - 6) * 6, (i - 5) * 6)

        return carry

    lax.fori_loop(0, 8, step, 0)
    expert_pair(7)
    sums_event(0)
    sums_event(1)

    for m in range(2, 7):
        attend(12 + (m - 2) * 4, 12 + (m - 1) * 4)
        sums_event(m)
    project()
    mix_event(0)
    mix_event(1)
    sums_final()
    for m in range(2, 7):
        mix_event(m)
    combine()
    mix_final()

    await_bytes(outgoing.at[pl.ds(0, 15)], out_sem.at[0])
    await_bytes(lg.at[0, pl.ds(0, 7)], out_sem.at[1])
    await_bytes(qg.at[0, pl.ds(0, 7)], out_sem.at[2])
    await_bytes(lg.at[pl.ds(0, 31)], out_sem.at[3])
    await_bytes(qg.at[0], out_sem.at[4])
    await_bytes(xg.at[pl.ds(0, 30)], out_sem.at[5])
    await_bytes(xg.at[pl.ds(0, 16)], out_sem.at[6])
    await_bytes(xg.at[pl.ds(0, 14)], out_sem.at[7])
    await_bytes(outgoing.at[pl.ds(0, 15)], out_sem.at[8])
    await_bytes(msg, out_sem.at[9])
    await_bytes(mp.at[pl.ds(0, 14)], out_sem.at[10])


def on_device(
    q_latent, kv_latent, rope_key, q_latent_gain, kv_latent_gain, w_query, w_key, w_value, query_gain, key_gain,
    w_mix, tokens_b, norm_gain, expert_ids, route_weights, w_gate, w_up, w_down,
):
    base, shift = rope_tables()

    def turn_gain(g):
        return jnp.concatenate([g[128:192], -g[160:192], g[128:160]])

    vec = jnp.concatenate(
        [
            q_latent_gain, kv_latent_gain, query_gain[:128], turn_gain(query_gain), key_gain[:128], turn_gain(key_gain),
            norm_gain,
        ]
    )[None, :]
    wq = jnp.concatenate([w_query, w_query[:, 160:192], w_query[:, 128:160]], axis=1)
    wkv = jnp.concatenate([w_key, w_value], axis=1)
    rope = jnp.concatenate([rope_key, rope_key[:, 32:], rope_key[:, :32]], axis=1)
    vmem = pl.BlockSpec(memory_space=pltpu.VMEM)
    hbm = pl.BlockSpec(memory_space=pl.ANY)
    dma = pltpu.SemaphoreType.DMA
    out = jax.ShapeDtypeStruct((48, 2048), BF16)
    return pl.pallas_call(
        layer,
        out_shape=(out, out),
        in_specs=[vmem] * 11 + [hbm] * 4,
        out_specs=(vmem, vmem),
        scratch_shapes=[
            pltpu.VMEM((128, 2048), BF16),
            pltpu.VMEM((2, 2048, 256), BF16),
            pltpu.VMEM((2, 2048, 256), BF16),
            pltpu.VMEM((2, 256, 2048), BF16),
            pltpu.VMEM((2, 8, 48, 384), BF16),
            pltpu.VMEM((768, 256), BF16),
            pltpu.VMEM((768, 256), F32),
            pltpu.VMEM((32, 8, 48, 384), BF16),
            pltpu.VMEM((2, 48, 128), BF16),
            pltpu.VMEM((16, 16, 1024), BF16),
            pltpu.VMEM((16, 16, 1024), BF16),
            pltpu.VMEM((16, 16, 1024), BF16),
            pltpu.VMEM((32, HALF, 2048), BF16),
            pltpu.VMEM((32, HALF, 2048), BF16),
            pltpu.VMEM((16, HALF, 2048), BF16),
            pltpu.VMEM((7, HALF, 2048), BF16),
            pltpu.VMEM((7, HALF, 2048), BF16),
            pltpu.VMEM((32, 48, 1024), BF16),
            pltpu.VMEM((16, 48, 1024), BF16),
            pltpu.VMEM((7, 48, 1024), BF16),
            pltpu.VMEM((7, 48, 1024), BF16),
            dma((4,)),
            dma((2,)),
            dma,
            dma((4,)),
            dma((4, 4)),
            dma,
            dma,
            dma,
            dma((7,)),
            dma((7,)),
            dma((2,)),
            dma((7,)),
            dma((7,)),
            dma((16,)),
            dma((7,)),
            dma((7,)),
            dma,
            dma((7,)),
            dma((7,)),
            dma((11,)),
        ],
        compiler_params=pltpu.CompilerParams(
            collective_id=0, has_side_effects=True, vmem_limit_bytes=67_043_328
        ),
    )(
        q_latent, kv_latent, rope, vec, wq, wkv, tokens_b, expert_ids, route_weights, jnp.asarray(base), jnp.asarray(shift),
        w_mix, w_gate, w_up, w_down,
    )


def solution(mesh):
    rows, whole = P(("ep", "tp"), None), P()
    in_specs = (
        rows, rows, rows, whole, whole, P(None, "tp"), P(None, "tp"), P(None, "tp"), whole, whole, P("tp", None), rows,
        whole, rows, rows, P("ep", None, "tp"), P("ep", None, "tp"), P("ep", "tp", None),
    )
    return jax.shard_map(on_device, mesh=mesh, in_specs=in_specs, out_specs=(rows, rows), check_vma=False)
```

time: 370 us -> 154 us (0.42)
  Pallas kernels: 0 us -> 139 us
  waiting for transfers between devices: 124 us -> 0 us
  matrix products: 67.5 us -> 0 us
  blocking collectives: 55.3 us -> 0 us
  local copies, waits for them, and re-layouts: 52.7 us -> 9.4 us
  other arithmetic: 39.8 us -> 4.56 us
  between operations: 14.1 us -> 0.65 us
  starting transfers between devices: 13.4 us -> 0 us
    pallas_call x0 -> x1, Pallas kernels: none -> 139 us  [on_device(): pl.pallas_call(layer, out_shape=(out, out), in_specs=[vmem] * 11 + [hbm]...]
    reduce_scatter x1 -> x0, waiting for transfers between devices: 74.4 us -> none  [one_scatter(): lax.psum_scatter(lines, axis, tiled=True).reshape(-1)]
    dot_general x10 -> x0, matrix products: 67.5 us -> none  [the longest x1 17.3 us: attention(): jnp.einsum('qhd,khd->hqk', queries, keys, preferred_element_type=jnp.floa...]
    all_gather x3 -> x0, blocking collectives: 55.3 us -> none  [the longest x1 22.4 us: on_device(): lax.all_gather(kv_normed[None], 'tp', axis=0, tiled=True)]
    all_gather x2 -> x0, waiting for transfers between devices: 42.8 us -> none  [the longest x1 42.8 us: sent_together(): whole, at, outs = (lax.all_gather(both, axis, axis=dim, tiled=True), 0, [])]
    concatenate x5 -> x3, other arithmetic: 25.6 us -> 3.73 us  [the longest x1 1.54 us: on_device(): wkv = jnp.concatenate([w_key, w_value], axis=1)]
    reshape x5 -> x0, local copies, waits for them, and re-layouts: 17.5 us -> none  [the longest x1 15.4 us: one_scatter(): jnp.pad(lines, ((0, 0), (0, rows * 128 - lines.shape[1]))).reshape(-1, 128)]
    all_to_all x2 -> x0, starting transfers between devices: 13.3 us -> none  [the longest x1 6.75 us: on_device(): lax.all_to_all(outgoing, 'ep', split_axis=0, concat_axis=0, tiled=True)]
  transfers between devices with their start and end apart: 5 -> 0, of which waited for: 3 -> 0; matrix products, arithmetic and copies ran while one was open for 23% -> 0% of each run, Pallas kernels for 0% -> 0%
where the time goes in v1:
time: 154 us
  Pallas kernels  139 us (90%)
  local copies, waits for them, and re-layouts  9.4 us (6%)
  other arithmetic  4.56 us (3%)
    pallas_call x1, Pallas kernels, on_device(): pl.pallas_call(layer, out_shape=(out, out), in_specs=[vmem] * 11 + [hbm]...  139 us
    unnamed x5, local copies, waits for them, and re-layouts  7 us

profile of v1, /device:TPU:1, one launch (start us, length us, event | category | flops | bytes accessed | tf_op | source)
XLA Modules:
  0.0 153.9 jit_solution(13643584971859836625)
XLA Ops:
  0.6 0.8 fusion.2
  1.5 0.8 concatenate.14
  2.3 0.6 broadcast_in_dim.3.vec_ref
  2.9 1.4 copy.25.ids_ref
  4.3 1.4 copy.26.route_ref
  5.6 0.9 fusion.1
  6.5 1.4 pad_maximum_fusion.2.rope_ref
  7.9 1.5 %pad_maximum_fusion.1.wkv_ref = bf16[256,256]{1,0:T(8,128)(2,1)} fusion(bf16[256,128]{1,0:T(8,128)(2,1)} %param.27, bf16[256,128]{1,0:T(8,128)(2,1)} %param.26), kind=kLoop, calls=%fused_computation.1 | loop fusion | flops 262144 | bytes 262144 | tf_op jit(solution)/shard_map/concatenate | solution.py:501
  9.4 1.0 copy.24
  10.5 0.1 fusion
  10.6 0.8 pad_maximum_fusion.wq_ref
  11.4 139.3 %shard_map.203 = (bf16[48,2048]{1,0:T(8,128)(2,1)}, bf16[48,2048]{1,0:T(8,128)(2,1)}) custom-call(bf16[48,384]{1,0:T(8,128)(2,1)} %ql_ref.1, bf16[48,256]{1,0:T(8,128)(2,1)} %kvl_ref.1, bf16[48,128]{1,0:T(8,128)(2,1)} %pad_maximum_fusion.2.rope_ref, f32[1,3200]{1,0:T(1,128)} %broadcast_in_dim.3.vec_ref, bf16[384,256]{1,0:T(8,128)(2,1)} %pad_maximum_fusion.wq_ref, ...), custom_call_target="tpu_custom_call" | custom-call | tf_op jit(solution)/shard_map/pallas_call | solution.py:507
  150.7 1.6 %copy.29 = bf16[48,2048]{1,0:T(8,128)(2,1)} copy(bf16[48,2048]{1,0:T(8,128)(2,1)} %get-tuple-element.14) | data formatting | bytes 393216
  152.3 1.6 %copy.30 = bf16[48,2048]{1,0:T(8,128)(2,1)} copy(bf16[48,2048]{1,0:T(8,128)(2,1)} %get-tuple-element.15) | data formatting | bytes 393216

commit v2 on v1

--- a/solution.py
+++ b/solution.py
@@ -15,6 +15,9 @@
 NT = (((1,), (1,)), ((), ()))
 TN = (((0,), (0,)), ((), ()))
 HALF = 64
+OFFSETS = (
+    (0, 0), (0, 1), (1, 0), (0, 3), (3, 0), (1, 1), (3, 3), (0, 2), (2, 0), (1, 3), (3, 1), (2, 1), (1, 2), (2, 3), (3, 2), (2, 2),
+)
 
 
 def rope_tables():
@@ -42,12 +45,17 @@
 
 
 def layer(
-    ql_ref, kvl_ref, rope_ref, vec_ref, wq_ref, wkv_ref, tokens_ref, ids_ref, route_ref, base_ref, shift_ref,
-    wmix_hbm, wg_hbm, wu_hbm, wd_hbm,
-    mix_ref, expert_ref,
-    wmix, wg, wu, wd, qg, queries, acc, lg, st, outgoing, arrived, returned, xg, pg, sg, rr, rl, mp, msg, mr, ml,
-    w_sem, z_sem, q_sib, la, lb, ls, a2a, ret, xr, xl, xs_own, xs_r, xs_l, sgs, rrs, rls, ms, mrs, mls, out_sem,
+    *refs,
 ):
+    inputs, (mix_ref, expert_ref), held = refs[:20], refs[20:22], refs[22:42]
+    (
+        tokens_ref, b_gain, ids_ref, ql_ref, kvl_ref, rope_ref, ql_gain, kvl_gain, q_gain, k_gain, base_ref, shift_ref,
+        wq_ref, wk_ref, wv_ref, route_ref, wg, wu, wd, wmix,
+    ) = held
+    (
+    wq, wkv, qg, queries, acc, lg, st, outgoing, arrived, returned, xg, pg, sg, rr, rl, mp, msg, mr, ml,
+    w_sem, z_sem, qr, ql, q_sib, la, lb, ls, a2a, ret, xr, xl, xs_own, xs_r, xs_l, sgs, rrs, rls, ms, mrs, mls, out_sem,
+    ) = refs[42:]
     e, t = lax.axis_index("ep"), lax.axis_index("tp")
     z, c = t // 2, t % 2
     other = 1 - c
@@ -60,6 +68,14 @@
     ey, ex = e // 4, e % 4
     pa = other * ex + c * ey
     pb = other * ey + c * ex
+
+    def away(n):
+        dy, dx = OFFSETS[n]
+        return ((ey + dy) % 4) * 4 + (ex + dx) % 4
+
+    def back_from(n):
+        dy, dx = OFFSETS[n]
+        return ((ey + 4 - dy) % 4) * 4 + (ex + 4 - dx) % 4
 
     def origin(da, db):
         a, b = (pa + da + 4) % 4, (pb + db + 4) % 4
@@ -72,31 +88,43 @@
         pl.semaphore_signal(barrier, inc=1, device_id=((e + d) % 16, t), device_id_type=MESH)
     pl.semaphore_signal(barrier, inc=1, device_id=sib, device_id_type=MESH)
 
-    loads = [
-        pltpu.make_async_copy(src, dst, w_sem.at[n])
-        for n, (src, dst) in enumerate([(wg_hbm, wg), (wu_hbm, wu), (wd_hbm, wd), (wmix_hbm, wmix)])
-    ]
-    for load in loads:
+    loads = [pltpu.make_async_copy(src, dst, w_sem.at[n]) for n, (src, dst) in enumerate(zip(inputs, held))]
+    for load in loads[:12]:
         load.start()
-
-    ids = ids_ref[...]
-    experts = lax.broadcasted_iota(jnp.int32, (48, 32), 1)
-    hot = [(ids[:, k : k + 1] == experts).astype(F32) for k in range(2)]
-    lower = (
-        lax.broadcasted_iota(jnp.int32, (48, 48), 0) > lax.broadcasted_iota(jnp.int32, (48, 48), 1)
-    ).astype(BF16)
+    for load in loads[:3]:
+        load.wait()
+
+    row48 = lax.broadcasted_iota(jnp.int32, (48, 48), 0)
+    col48 = lax.broadcasted_iota(jnp.int32, (48, 48), 1)
+
+    def column(x):
+        return jnp.sum(jnp.where(row48 == col48, x, 0.0), axis=1, keepdims=True)
+
+    ids = [column(ids_ref[k : k + 1].astype(F32)) for k in range(2)]
+    place32 = lax.broadcasted_iota(jnp.int32, (1, 32), 1)
+    experts = place32 % 2 * 1.0
+    for n in range(16):
+        experts += jnp.where(place32 // 2 == n, (away(n) * 2).astype(F32), 0.0)
+    first_slot = (place32 * 4).astype(F32)
+    hot = [(ids[k] == experts).astype(F32) for k in range(2)]
+    lower = (row48 > col48).astype(BF16)
     before = [jnp.dot(lower, h.astype(BF16), preferred_element_type=F32) for h in hot]
     before[1] = before[1] + jnp.sum(hot[0], axis=0, keepdims=True)
     places = lax.broadcasted_iota(jnp.int32, (48, 128), 1).astype(F32)
     for k in range(2):
         rank = jnp.sum(hot[k] * before[k], axis=1, keepdims=True)
-        slot = ids[:, k : k + 1].astype(F32) * 4.0 + rank
+        slot = jnp.sum(hot[k] * first_slot, axis=1, keepdims=True) + rank
         st[k] = (slot == places).astype(BF16)
-    b_normed = normed(tokens_ref[...].astype(F32), vec_ref[:, 1152:3200]).astype(BF16)
+    b_normed = normed(tokens_ref[...].astype(F32), b_gain[...].reshape(1, 2048)).astype(BF16)
     slots = lax.dot_general(st[0] + st[1], b_normed, TN, preferred_element_type=F32)
     slots = slots.reshape(16, 8, 2048)
     outgoing[...] = jnp.concatenate([slots[:, :, :1024], slots[:, :, 1024:]], axis=1).astype(BF16)
 
+    for load in loads[12:]:
+        load.start()
+    for load in loads[3:12]:
+        load.wait()
+
     trig_q = shift_ref[pl.ds(e, 1), 0], shift_ref[pl.ds(e, 1), 1]
     lane = lax.broadcasted_iota(jnp.int32, (1, 128), 1)
     flip = jnp.where(lane < 64, -1.0, 1.0)
@@ -104,14 +132,23 @@
     def turning(u, gains):
         return (trig_q[0] * u + trig_q[1] * (pltpu.roll(u, 64, axis=1) * flip)) * gains
 
+    def swapped(v):
+        return jnp.concatenate([v, v[:, 32:64], v[:, 0:32]], axis=1)
+
+    def turn_gain(g):
+        tail = g[:, 128:192]
+        return swapped(tail) * jnp.where((lane >= 64) & (lane < 96), -1.0, 1.0)
+
+    gq, kg = q_gain[...].reshape(1, 192), k_gain[...].reshape(1, 192)
+
     def turned(v):
         return v + pltpu.roll(v, 64, axis=1)
 
-    qg[c, z] = normed(ql_ref[...].astype(F32), vec_ref[:, 0:384]).astype(BF16)
+    qg[c, z] = normed(ql_ref[...].astype(F32), ql_gain[...].reshape(1, 384)).astype(BF16)
     mine = lg.at[e * 2 + c, z]
-    mine[:, 0:256] = normed(kvl_ref[...].astype(F32), vec_ref[:, 384:640]).astype(BF16)
-    rope = rope_ref[...].astype(F32)
-    rope_rot = turned(rope * turning(base_ref[c * 8 + z], vec_ref[:, 1024:1152]))
+    mine[:, 0:256] = normed(kvl_ref[...].astype(F32), kvl_gain[...].reshape(1, 256)).astype(BF16)
+    rope = swapped(rope_ref[...].astype(F32))
+    rope_rot = turned(rope * turning(base_ref[c * 8 + z], turn_gain(kg)))
     squares = jnp.sum(jnp.where(lane < 64, rope * rope, 0.0), axis=1, keepdims=True)
     high = squares.astype(BF16).astype(F32)
     mine[:, 256:384] = jnp.where(
@@ -119,14 +156,11 @@
     ).astype(BF16)
 
     pl.semaphore_wait(barrier, 23)
-    for d in range(1, 16):
-        peer = (e + d) % 16
-        send(outgoing.at[peer], arrived.at[e], out_sem.at[0], a2a, (peer, t))
+    for n in range(1, 16):
+        send(outgoing.at[n], arrived.at[n], out_sem.at[0], a2a.at[n // 8], (away(n), t))
     for d in range(1, 8):
-        send(mine, mine, out_sem.at[1], z_sem.at[0], zpeer(d))
-    for d in range(1, 8):
-        send(qg.at[c, z], qg.at[c, z], out_sem.at[2], z_sem.at[1], zpeer(d))
-    arrived[pl.ds(e, 1)] = outgoing[pl.ds(e, 1)]
+        send(mine, mine, out_sem.at[1], z_sem, zpeer(d))
+    arrived[0] = outgoing[0]
 
     a_up, a_down = (origin(1, 0), t), (origin(-1, 0), t)
     b_up, b_down = (origin(0, 1), t), (origin(0, -1), t)
@@ -146,7 +180,7 @@
         full(block(da, 0), ls, sib)
 
     def start_latents():
-        await_bytes(lg.at[0, pl.ds(0, 7)], z_sem.at[0])
+        await_bytes(lg.at[0, pl.ds(0, 7)], z_sem)
         full(block(0, 0), la.at[0], a_up)
         full(block(0, 0), la.at[1], a_down)
         along_b(0, 0)
@@ -179,23 +213,42 @@
         await_bytes(part(da, 2, 1), lb.at[n, 3])
         full(block(da, 2), ls, sib)
 
-    def start_queries():
-        await_bytes(qg.at[0, pl.ds(0, 7)], z_sem.at[1])
-        send(qg.at[c], qg.at[c], out_sem.at[4], q_sib, sib)
+    def relay_queries(i):
+        from_left, from_right = qg.at[c, (z + 8 - i) % 8], qg.at[c, (z + i) % 8]
+
+        @pl.when((i >= 1) & (i <= 4))
+        def _():
+            await_bytes(from_left, qr.at[i - 1])
+
+        @pl.when((i >= 1) & (i <= 3))
+        def _():
+            await_bytes(from_right, ql.at[i - 1])
+
+        @pl.when(i <= 3)
+        def _():
+            send(from_left, from_left, out_sem.at[2], qr.at[i], right)
+
+        @pl.when(i <= 2)
+        def _():
+            send(from_right, from_right, out_sem.at[2], ql.at[i], left)
+
+        @pl.when(i == 4)
+        def _():
+            send(qg.at[c], qg.at[c], out_sem.at[4], q_sib, sib)
 
     def make_queries():
         await_bytes(qg.at[0], q_sib)
 
         def rows(n, carry):
             x = qg[n // 2, pl.ds((n % 2) * 4, 4)].reshape(192, 384)
-            p = jnp.dot(x, wq_ref[...], preferred_element_type=F32)
+            p = lax.dot_general(x, wq[...], NT, preferred_element_type=F32)
             nope, rot = p[:, :128], p[:, 128:]
             total = jnp.sum(nope * nope + jnp.where(lane < 64, rot * rot, 0.0), axis=1, keepdims=True)
             scale = lax.rsqrt(total * (1.0 / 192.0) + EPSILON) * (SCORE * LOG2E)
-            angles = turning(base_ref[pl.ds(n * 4, 4)].reshape(192, 128), vec_ref[:, 768:896])
+            angles = turning(base_ref[pl.ds(n * 4, 4)].reshape(192, 128), turn_gain(gq))
             rot = jnp.where(lane < 64, turned(rot * angles), 0.0) * scale
             at = pl.ds(pl.multiple_of(n * 192, 192), 192)
-            queries[at, 0:128] = (nope * vec_ref[:, 640:768] * scale).astype(BF16)
+            queries[at, 0:128] = (nope * gq[:, :128] * scale).astype(BF16)
             queries[at, 128:256] = rot.astype(BF16)
             acc[at] = jnp.zeros((192, 256), F32)
             return carry
@@ -204,16 +257,16 @@
 
     def attend(first, last):
         def keys_of(n, carry):
-            rows = lg[n].reshape(384, 384)
-            kv = jnp.dot(rows[:, :256], wkv_ref[...], preferred_element_type=F32)
+            rows = lg[pl.ds(n * 2, 2)].reshape(768, 384)
+            kv = jnp.dot(rows[:, :256], wkv[...], preferred_element_type=F32)
             tail = rows[:, 256:].astype(F32)
             nope = kv[:, :128]
             total = jnp.sum(nope * nope + jnp.where(lane < 64, 0.0, tail), axis=1, keepdims=True)
             scale = lax.rsqrt(total * (1.0 / 192.0) + EPSILON)
             keys = jnp.concatenate(
-                [nope * (vec_ref[:, 896:1024] * scale), jnp.where(lane < 64, tail, 0.0) * scale], axis=1
+                [nope * (kg[:, :128] * scale), jnp.where(lane < 64, tail, 0.0) * scale], axis=1
             ).astype(BF16)
-            values = jnp.concatenate([kv[:, 128:].astype(BF16), jnp.ones((384, 128), BF16)], axis=1)
+            values = jnp.concatenate([kv[:, 128:].astype(BF16), jnp.ones((768, 128), BF16)], axis=1)
             for m in range(3):
                 at = pl.ds(m * 256, 256)
                 scores = lax.dot_general(queries[at], keys, NT, preferred_element_type=F32)
@@ -228,21 +281,19 @@
     def xsend(ref, sem, device):
         send(ref, ref, out_sem.at[5], sem, device)
 
-    def settle():
-        await_bytes(outgoing.at[pl.ds(0, 15)], a2a)
-        row = lax.broadcasted_iota(jnp.int32, (128, 128), 0)
-        col = lax.broadcasted_iota(jnp.int32, (128, 128), 1)
-        moved = (row == (col % 8 // 4) * 64 + col // 8 * 4 + col % 4).astype(BF16)
-        came = arrived[...].astype(F32)
+    def settle(g):
+        await_bytes(outgoing.at[pl.ds(0, 7 + g)], a2a.at[g])
+        row = lax.broadcasted_iota(jnp.int32, (HALF, HALF), 0)
+        col = lax.broadcasted_iota(jnp.int32, (HALF, HALF), 1)
+        moved = (row == (col % 8 // 4) * 32 + col // 8 * 4 + col % 4).astype(BF16)
+        came = arrived[g * 8 : g * 8 + 8].astype(F32)
+        own = xblock(z, g, c)
         for n in range(2):
-            piece = came[:, n * 8 : n * 8 + 8].reshape(128, 1024).astype(BF16)
-            piece = jnp.dot(moved, piece, preferred_element_type=F32).astype(BF16)
-            for h in range(2):
-                xg[(z * 2 + h) * 2 + c, :, n * 1024 : n * 1024 + 1024] = piece[h * HALF : h * HALF + HALF]
-        for h in range(2):
-            xsend(xblock(z, h, c), xr.at[h], right)
-            xsend(xblock(z, h, c), xl.at[h], left)
-            xsend(xblock(z, h, c), xs_own.at[h], sib)
+            piece = came[:, n * 8 : n * 8 + 8].reshape(HALF, 1024).astype(BF16)
+            own[:, n * 1024 : n * 1024 + 1024] = jnp.dot(moved, piece, preferred_element_type=F32).astype(BF16)
+        xsend(own, xr.at[g], right)
+        xsend(own, xl.at[g], left)
+        xsend(own, xs_own.at[g], sib)
 
     def relay_rows(j):
         k, hr = j // 2 + 1, j % 2
@@ -267,41 +318,43 @@
 
         xsend(from_right, xs_l.at[j], sib)
 
-    def expert(zo, h, sem):
-        x = xg[pl.ds((zo * 2 + h) * 2, 2)].reshape(128, 2048)
-        gate = jnp.dot(x, wg[h], preferred_element_type=F32)
-        up = jnp.dot(x, wu[h], preferred_element_type=F32)
-        hidden = (gate / (1.0 + jnp.exp(-gate)) * up).astype(BF16)
-        for n in range(4):
-            cols = pl.ds(n * 512, 512)
-            y = jnp.dot(hidden, wd[h, :, cols], preferred_element_type=F32).astype(BF16)
-            pg[zo * 2 + h, :, cols] = y[:HALF]
-            pg[16 + zo * 2 + h, :, cols] = y[HALF:]
-        send(pg.at[other * 16 + zo * 2 + h], sg.at[zo * 2 + h], out_sem.at[6], sem, sib)
-
     def expert_pair(i):
         j = i - 1
+        started = (i + 7) // 8
         k = (j + 2) // 2
-        h0 = (1 - (i + 7) // 8) * 0 + ((i + 7) // 8) * (j + 2) % 2
-        started = (i + 7) // 8
+        g0 = started * ((j + 2) % 2)
+        g1 = (1 - started) + started * (g0 + i // 7)
+        n0 = ((z + started * (8 - k)) % 8) * 2 + g0
+        n1 = ((z + started * k) % 8) * 2 + g1
 
         @pl.when(i == 0)
         def _():
-            await_bytes(xblock(z, 0, other), xs_own.at[0])
-            await_bytes(xblock(z, 1, other), xs_own.at[1])
+            await_bytes(xg.at[0], xs_own.at[0])
+            await_bytes(xg.at[0], xs_own.at[1])
 
         @pl.when(i > 0)
         def _():
-            await_bytes(xblock((z - k + 8) % 8, 0, other), xs_r.at[j])
-            await_bytes(xblock((z + k) % 8, 0, other), xs_l.at[j])
-
-        def one(s, carry):
-            zo = (z + started * (s * k + (1 - s) * (8 - k))) % 8
-            hs = (1 - started) * s + started * (h0 + s * (i // 7))
-            expert(zo, hs, sgs.at[i * 2 + s])
+            await_bytes(xg.at[0], xs_r.at[j])
+            await_bytes(xg.at[0], xs_l.at[j])
+
+        def one(h, carry):
+            at = pl.ds(pl.multiple_of(h * 32, 32), 32)
+            x = jnp.concatenate([xg[n0 * 2, at], xg[n0 * 2 + 1, at], xg[n1 * 2, at], xg[n1 * 2 + 1, at]], axis=0)
+            gate = jnp.dot(x, wg[h], preferred_element_type=F32)
+            up = jnp.dot(x, wu[h], preferred_element_type=F32)
+            hidden = (gate / (1.0 + jnp.exp(-gate)) * up).astype(BF16)
+            for n in range(4):
+                cols = pl.ds(n * 512, 512)
+                y = jnp.dot(hidden, wd[h, :, cols], preferred_element_type=F32).astype(BF16)
+                pg[n0, at, cols] = y[0:32]
+                pg[16 + n0, at, cols] = y[32:64]
+                pg[n1, at, cols] = y[64:96]
+                pg[16 + n1, at, cols] = y[96:128]
             return carry
 
         lax.fori_loop(0, 2, one, 0)
+        send(pg.at[other * 16 + n0], sg.at[n0], out_sem.at[6], sgs.at[i * 2], sib)
+        send(pg.at[other * 16 + n1], sg.at[n1], out_sem.at[6], sgs.at[i * 2 + 1], sib)
 
     def add_rows(out, terms, rows):
         def tile(n, carry):
@@ -314,7 +367,7 @@
 
         lax.fori_loop(0, rows // 16, tile, 0)
 
-    def sums_event(m):
+    def sums_event(m, first, last):
         k = 4 - (m + 1) // 2
         for side in range(2):
             h = m % 2 if side == 0 else 1 - m % 2
@@ -329,6 +382,9 @@
                 terms.append(recv.at[m - 2])
             add_rows(mine_, terms, HALF)
             send(mine_, recv.at[m], out_sem.at[7], sems.at[m], device)
+            if last > first:
+                middle = (first + last) // 2
+                attend(*((first, middle), (middle, last))[side])
 
     def sums_final():
         for h in range(2):
@@ -337,16 +393,15 @@
             await_bytes(rl.at[5 + h], rls.at[5 + h])
             own = pg.at[c * 16 + z * 2 + h]
             add_rows(own, [own, sg.at[z * 2 + h], rr.at[6 - h], rl.at[5 + h]], HALF)
-        row = lax.broadcasted_iota(jnp.int32, (128, 128), 0)
-        col = lax.broadcasted_iota(jnp.int32, (128, 128), 1)
-        back = (col == (row % 8 // 4) * 64 + row // 8 * 4 + row % 4).astype(BF16)
-        done = pg[pl.ds(c * 16 + z * 2, 2)].reshape(128, 2048)
-        rows = jnp.dot(back, done, preferred_element_type=F32).reshape(16, 8, 2048)
-        arrived[...] = jnp.concatenate([rows[:, :, :1024], rows[:, :, 1024:]], axis=1).astype(BF16)
-        for d in range(1, 16):
-            peer = (e + d) % 16
-            send(arrived.at[peer], returned.at[e], out_sem.at[8], ret, (peer, t))
-        returned[pl.ds(e, 1)] = arrived[pl.ds(e, 1)]
+        row = lax.broadcasted_iota(jnp.int32, (HALF, HALF), 0)
+        col = lax.broadcasted_iota(jnp.int32, (HALF, HALF), 1)
+        back = (col == (row % 8 // 4) * 32 + row // 8 * 4 + row % 4).astype(BF16)
+        for g in range(2):
+            rows = jnp.dot(back, pg[c * 16 + z * 2 + g], preferred_element_type=F32).reshape(8, 8, 2048)
+            arrived[g * 8 : g * 8 + 8] = jnp.concatenate([rows[:, :, :1024], rows[:, :, 1024:]], axis=1).astype(BF16)
+        for n in range(1, 16):
+            send(arrived.at[n], returned.at[n], out_sem.at[8], ret, (back_from(n), t))
+        returned[0] = arrived[0]
 
     def project():
         def piece(n, carry):
@@ -398,68 +453,71 @@
             piece = came[:, n * 8 : n * 8 + 8].reshape(128, 1024).astype(BF16)
             total = jnp.zeros((48, 1024), F32)
             for k in range(2):
-                total += jnp.dot(st[k], piece, preferred_element_type=F32) * route_ref[:, k : k + 1]
+                total += jnp.dot(st[k], piece, preferred_element_type=F32) * column(route_ref[k : k + 1])
             expert_ref[:, n * 1024 : n * 1024 + 1024] = total.astype(BF16)
 
+    relay_queries(0)
+    settle(0)
+    settle(1)
     start_latents()
-    start_queries()
-    settle()
-    for load in loads:
+    for load in loads[12:]:
         load.wait()
+    wq[0:192] = wq_ref[...]
+    wq[192:224] = wq_ref[160:192]
+    wq[224:256] = wq_ref[128:160]
+    wkv[:, 0:128] = wk_ref[...]
+    wkv[:, 128:256] = wv_ref[...]
 
     def step(i, carry):
-        @pl.when(i == 0)
+        @pl.when(i == 1)
         def _():
             relay_a()
-            make_queries()
-
-        @pl.when(i > 0)
-        def _():
-            relay_rows(i - 1)
-
-        @pl.when(i == 1)
+
+        @pl.when(i == 2)
         def _():
             relay_a_far()
             relay_b(0)
 
-        @pl.when(i == 2)
+        @pl.when(i == 3)
         def _():
             relay_b_far(0)
             relay_b(1)
 
+        @pl.when(i == 4)
+        def _():
+            relay_b_far(2)
+            relay_b(3)
+
+        @pl.when(i == 5)
+        def _():
+            relay_b_far(3)
+            make_queries()
+            await_bytes(lg.at[pl.ds(0, 16)], ls)
+
+        @pl.when((i >= 1) & (i <= 4))
+        def _():
+            relay_queries(i)
+
+        expert_pair(i)
+
         @pl.when(i == 3)
         def _():
             relay_b_far(1)
             relay_b(2)
 
-        @pl.when(i == 4)
-        def _():
-            relay_b_far(2)
-            relay_b(3)
-
-        @pl.when(i == 5)
-        def _():
-            relay_b_far(3)
-            await_bytes(lg.at[pl.ds(0, 16)], ls)
-
-        @pl.when(i > 0)
-        def _():
-            expert_pair(i - 1)
-
-        @pl.when(i >= 6)
-        def _():
-            attend((i - 6) * 6, (i - 5) * 6)
-
+        @pl.when(i >= 5)
+        def _():
+            attend((i - 5) * 2, (i - 4) * 2)
+
+        relay_rows(i)
         return carry
 
-    lax.fori_loop(0, 8, step, 0)
+    lax.fori_loop(0, 7, step, 0)
     expert_pair(7)
-    sums_event(0)
-    sums_event(1)
-
+    sums_event(0, 0, 0)
+    sums_event(1, 0, 0)
     for m in range(2, 7):
-        attend(12 + (m - 2) * 4, 12 + (m - 1) * 4)
-        sums_event(m)
+        sums_event(m, 4 + (m - 2) * 12 // 5, 4 + (m - 1) * 12 // 5)
     project()
     mix_event(0)
     mix_event(1)
@@ -487,33 +545,24 @@
     w_mix, tokens_b, norm_gain, expert_ids, route_weights, w_gate, w_up, w_down,
 ):
     base, shift = rope_tables()
-
-    def turn_gain(g):
-        return jnp.concatenate([g[128:192], -g[160:192], g[128:160]])
-
-    vec = jnp.concatenate(
-        [
-            q_latent_gain, kv_latent_gain, query_gain[:128], turn_gain(query_gain), key_gain[:128], turn_gain(key_gain),
-            norm_gain,
-        ]
-    )[None, :]
-    wq = jnp.concatenate([w_query, w_query[:, 160:192], w_query[:, 128:160]], axis=1)
-    wkv = jnp.concatenate([w_key, w_value], axis=1)
-    rope = jnp.concatenate([rope_key, rope_key[:, 32:], rope_key[:, :32]], axis=1)
+    operands = (
+        tokens_b, norm_gain, expert_ids.T, q_latent, kv_latent, rope_key, q_latent_gain, kv_latent_gain, query_gain,
+        key_gain, jnp.asarray(base), jnp.asarray(shift), w_query.T, w_key, w_value, route_weights.T, w_gate, w_up, w_down,
+        w_mix,
+    )
     vmem = pl.BlockSpec(memory_space=pltpu.VMEM)
     hbm = pl.BlockSpec(memory_space=pl.ANY)
     dma = pltpu.SemaphoreType.DMA
     out = jax.ShapeDtypeStruct((48, 2048), BF16)
-    return pl.pallas_call(
+    results = pl.pallas_call(
         layer,
         out_shape=(out, out),
-        in_specs=[vmem] * 11 + [hbm] * 4,
+        in_specs=[hbm] * 20,
         out_specs=(vmem, vmem),
         scratch_shapes=[
-            pltpu.VMEM((128, 2048), BF16),
-            pltpu.VMEM((2, 2048, 256), BF16),
-            pltpu.VMEM((2, 2048, 256), BF16),
-            pltpu.VMEM((2, 256, 2048), BF16),
+            *[pltpu.VMEM(a.shape, a.dtype) for a in operands],
+            pltpu.VMEM((256, 384), BF16),
+            pltpu.VMEM((256, 256), BF16),
             pltpu.VMEM((2, 8, 48, 384), BF16),
             pltpu.VMEM((768, 256), BF16),
             pltpu.VMEM((768, 256), F32),
@@ -531,13 +580,15 @@
             pltpu.VMEM((16, 48, 1024), BF16),
             pltpu.VMEM((7, 48, 1024), BF16),
             pltpu.VMEM((7, 48, 1024), BF16),
+            dma((20,)),
+            dma,
             dma((4,)),
-            dma((2,)),
+            dma((3,)),
             dma,
             dma((4,)),
             dma((4, 4)),
             dma,
-            dma,
+            dma((2,)),
             dma,
             dma((7,)),
             dma((7,)),
@@ -555,10 +606,13 @@
         compiler_params=pltpu.CompilerParams(
             collective_id=0, has_side_effects=True, vmem_limit_bytes=67_043_328
         ),
-    )(
-        q_latent, kv_latent, rope, vec, wq, wkv, tokens_b, expert_ids, route_weights, jnp.asarray(base), jnp.asarray(shift),
-        w_mix, w_gate, w_up, w_down,
-    )
+    )(*operands)
+    return pl.pallas_call(hand_over, out_shape=(out, out), in_specs=[vmem] * 2, out_specs=(vmem, vmem))(*results)
+
+
+def hand_over(mix_ref, expert_ref, mix_out, expert_out):
+    mix_out[...] = mix_ref[...]
+    expert_out[...] = expert_ref[...]
 
 
 def solution(mesh):

time: 154 us -> 135 us (0.88)
  local copies, waits for them, and re-layouts: 9.4 us -> 0 us
  Pallas kernels: 139 us -> 134 us
  other arithmetic: 4.56 us -> 0 us
    unnamed x5 -> x0, local copies, waits for them, and re-layouts: 7 us -> none
    pallas_call x1 -> x2, Pallas kernels: 139 us -> 134 us  [the longest x1 132 us: on_device(): pl.pallas_call(layer, out_shape=(out, out), in_specs=[hbm] * 20, out_spec...]
    concatenate x3 -> x0, other arithmetic: 3.73 us -> none  [the longest x1 1.54 us: on_device(): wkv = jnp.concatenate([w_key, w_value], axis=1)]
where the time goes in v2:
time: 135 us
  Pallas kernels  134 us (99%)
    pallas_call x1, Pallas kernels, on_device(): pl.pallas_call(layer, out_shape=(out, out), in_specs=[hbm] * 20, out_spec...  132 us

profile of v2, /device:TPU:1, one launch (start us, length us, event | category | flops | bytes accessed | tf_op | source)
XLA Modules:
  0.0 134.6 jit_solution(8861656200799286067)
XLA Ops:
  0.6 132.1 %shard_map.203 = (bf16[48,2048]{1,0:T(8,128)(2,1)}, bf16[48,2048]{1,0:T(8,128)(2,1)}) custom-call(bf16[48,2048]{1,0:T(8,128)(2,1)} %refs_0_.1, f32[2048]{0:T(1024)} %refs_1_.1, s32[2,48]{1,0:T(2,128)} %bitcast.4, bf16[48,384]{1,0:T(8,128)(2,1)} %refs_3_.1, bf16[48,256]{1,0:T(8,128)(2,1)} %refs_4_.1, bf16[48,64]{1,0:T(8,128)(2,1)} %refs_5_.1, f32[384]{0:T(512)} %refs_6_.1, ...), custom_call_target="tpu_custom_call" | custom-call | tf_op jit(solution)/shard_map/pallas_call | solution.py:557
  132.8 1.8 %shard_map.204 = (bf16[48,2048]{1,0:T(8,128)(2,1)}, bf16[48,2048]{1,0:T(8,128)(2,1)}) custom-call(bf16[48,2048]{1,0:T(8,128)(2,1)} %get-tuple-element.4.mix_ref, bf16[48,2048]{1,0:T(8,128)(2,1)} %get-tuple-element.5.expert_ref), custom_call_target="tpu_custom_call" | custom-call | tf_op jit(solution)/shard_map/pallas_call | solution.py:610

commit v3 on v2

--- a/solution.py
+++ b/solution.py
@@ -458,8 +458,8 @@
 
     relay_queries(0)
     settle(0)
+    start_latents()
     settle(1)
-    start_latents()
     for load in loads[12:]:
         load.wait()
     wq[0:192] = wq_ref[...]
@@ -472,42 +472,34 @@
         @pl.when(i == 1)
         def _():
             relay_a()
+            relay_b(0)
 
         @pl.when(i == 2)
         def _():
             relay_a_far()
-            relay_b(0)
 
         @pl.when(i == 3)
         def _():
-            relay_b_far(0)
             relay_b(1)
 
         @pl.when(i == 4)
         def _():
-            relay_b_far(2)
+            relay_b(2)
+
+        @pl.when(i == 5)
+        def _():
             relay_b(3)
 
-        @pl.when(i == 5)
-        def _():
-            relay_b_far(3)
+        @pl.when((i >= 1) & (i <= 4))
+        def _():
+            relay_queries(i)
+
+        expert_pair(i)
+
+        @pl.when(i == 6)
+        def _():
             make_queries()
-            await_bytes(lg.at[pl.ds(0, 16)], ls)
-
-        @pl.when((i >= 1) & (i <= 4))
-        def _():
-            relay_queries(i)
-
-        expert_pair(i)
-
-        @pl.when(i == 3)
-        def _():
-            relay_b_far(1)
-            relay_b(2)
-
-        @pl.when(i >= 5)
-        def _():
-            attend((i - 5) * 2, (i - 4) * 2)
+            sums_event(1, 0, 0)
 
         relay_rows(i)
         return carry
@@ -515,10 +507,13 @@
     lax.fori_loop(0, 7, step, 0)
     expert_pair(7)
     sums_event(0, 0, 0)
-    sums_event(1, 0, 0)
-    for m in range(2, 7):
-        sums_event(m, 4 + (m - 2) * 12 // 5, 4 + (m - 1) * 12 // 5)
+    for n in range(4):
+        relay_b_far(n)
+    await_bytes(lg.at[pl.ds(0, 16)], ls)
+    for n, m in enumerate((3, 2, 5, 4)):
+        sums_event(m, n * 4, n * 4 + 4)
     project()
+    sums_event(6, 0, 0)
     mix_event(0)
     mix_event(1)
     sums_final()

time: 135 us -> 125 us (0.926)
  Pallas kernels: 134 us -> 123 us
    pallas_call x1, Pallas kernels: 132 us -> 121 us  [on_device(): pl.pallas_call(layer, out_shape=(out, out), in_specs=[hbm] * 20, out_spec...]
where the time goes in v3:
time: 125 us; the launch traced here: 124 us
  Pallas kernels  123 us (98%)
    pallas_call x1, Pallas kernels, on_device(): pl.pallas_call(layer, out_shape=(out, out), in_specs=[hbm] * 20, out_spec...  121 us

profile of v3, /device:TPU:1, one launch (start us, length us, event | category | flops | bytes accessed | tf_op | source)
XLA Modules:
  0.0 123.6 jit_solution(2989190210021865761)
XLA Ops:
  0.6 121.2 %shard_map.203 = (bf16[48,2048]{1,0:T(8,128)(2,1)}, bf16[48,2048]{1,0:T(8,128)(2,1)}) custom-call(bf16[48,2048]{1,0:T(8,128)(2,1)} %refs_0_.1, f32[2048]{0:T(1024)} %refs_1_.1, s32[2,48]{1,0:T(2,128)} %bitcast.4, bf16[48,384]{1,0:T(8,128)(2,1)} %refs_3_.1, bf16[48,256]{1,0:T(8,128)(2,1)} %refs_4_.1, bf16[48,64]{1,0:T(8,128)(2,1)} %refs_5_.1, f32[384]{0:T(512)} %refs_6_.1, ...), custom_call_target="tpu_custom_call" | custom-call | tf_op jit(solution)/shard_map/pallas_call | solution.py:552
  121.9 1.8 %shard_map.204 = (bf16[48,2048]{1,0:T(8,128)(2,1)}, bf16[48,2048]{1,0:T(8,128)(2,1)}) custom-call(bf16[48,2048]{1,0:T(8,128)(2,1)} %get-tuple-element.4.mix_ref, bf16[48,2048]{1,0:T(8,128)(2,1)} %get-tuple-element.5.expert_ref), custom_call_target="tpu_custom_call" | custom-call | tf_op jit(solution)/shard_map/pallas_call | solution.py:605

commit v4 on v3

--- a/solution.py
+++ b/solution.py
@@ -513,11 +513,12 @@
     for n, m in enumerate((3, 2, 5, 4)):
         sums_event(m, n * 4, n * 4 + 4)
     project()
+    mix_event(0)
     sums_event(6, 0, 0)
-    mix_event(0)
     mix_event(1)
+    mix_event(2)
     sums_final()
-    for m in range(2, 7):
+    for m in range(3, 7):
         mix_event(m)
     combine()
     mix_final()

time: 125 us -> 126 us (level)
  Pallas kernels: 123 us -> 125 us
    pallas_call x1, Pallas kernels: 121 us -> 123 us  [on_device(): pl.pallas_call(layer, out_shape=(out, out), in_specs=[hbm] * 20, out_spec...]
where the time goes in v4:
time: 126 us
  Pallas kernels  125 us (99%)
    pallas_call x1, Pallas kernels, on_device(): pl.pallas_call(layer, out_shape=(out, out), in_specs=[hbm] * 20, out_spec...  123 us

profile of v4, /device:TPU:1, one launch (start us, length us, event | category | flops | bytes accessed | tf_op | source)
XLA Modules:
  0.0 125.6 jit_solution(47617991647700378)
XLA Ops:
  0.6 123.2 %shard_map.203 = (bf16[48,2048]{1,0:T(8,128)(2,1)}, bf16[48,2048]{1,0:T(8,128)(2,1)}) custom-call(bf16[48,2048]{1,0:T(8,128)(2,1)} %refs_0_.1, f32[2048]{0:T(1024)} %refs_1_.1, s32[2,48]{1,0:T(2,128)} %bitcast.4, bf16[48,384]{1,0:T(8,128)(2,1)} %refs_3_.1, bf16[48,256]{1,0:T(8,128)(2,1)} %refs_4_.1, bf16[48,64]{1,0:T(8,128)(2,1)} %refs_5_.1, f32[384]{0:T(512)} %refs_6_.1, ...), custom_call_target="tpu_custom_call" | custom-call | tf_op jit(solution)/shard_map/pallas_call | solution.py:553
  123.9 1.8 %shard_map.204 = (bf16[48,2048]{1,0:T(8,128)(2,1)}, bf16[48,2048]{1,0:T(8,128)(2,1)}) custom-call(bf16[48,2048]{1,0:T(8,128)(2,1)} %get-tuple-element.4.mix_ref, bf16[48,2048]{1,0:T(8,128)(2,1)} %get-tuple-element.5.expert_ref), custom_call_target="tpu_custom_call" | custom-call | tf_op jit(solution)/shard_map/pallas_call | solution.py:606
